TPU v7x, 32 devices: a whole 2x2x4 slice. The times are simulated.
32 devices in a mesh: sp: 8 (over z, core), tp: 4 (over y, x).
Axes of the slice: x: 2, y: 2, z: 4, core: 2. Of those that a mesh axis runs over, the one named last changes fastest.
Arguments:
- residual_in: bfloat16 [2048, 2048], P(('sp', 'tp')), may hold values from -6 to 6
- query_a: bfloat16 [2048, 1024], P('sp', 'tp'), may hold values from -12 to 12
- key_a: bfloat16 [2048, 1024], P('sp', 'tp'), may hold values from -12 to 12
- value_a: bfloat16 [2048, 1024], P('sp', 'tp'), may hold values from -6 to 6
- query_b: bfloat16 [2048, 2048], P('sp', 'tp'), may hold values from -12 to 12
- key_b: bfloat16 [2048, 2048], P('sp', 'tp'), may hold values from -12 to 12
- value_b: bfloat16 [2048, 2048], P('sp', 'tp'), may hold values from -6 to 6
- cum_gates: float32 [2048, 2, 16], P('sp', None, 'tp'), may hold values from -247.76 to 0, as said below
- out_a: bfloat16 [1024, 2048], P('tp'), may hold values from -0.1875 to 0.1875
- out_b: bfloat16 [2048, 2048], P('tp'), may hold values from -0.125 to 0.125
- post_gain: bfloat16 [2048], replicated, may hold values from 0.099609375 to 1.8984375
- pre_gain: bfloat16 [2048], replicated, may hold values from 0.099609375 to 1.8984375
- expert_ids: int32 [2048, 2], P('sp'), may hold values from 0 to 7, all different within a row; in each aligned block of 256 rows (0 to 255, 256 to 511, ...) at most 80 rows name the same one
- expert_weights: float32 [2048, 2], P('sp'), may hold values from 0.2 to 1
- w_gate: bfloat16 [8, 2048, 4096], P('sp', None, 'tp'), may hold values from -0.125 to 0.125
- w_up: bfloat16 [8, 2048, 4096], P('sp', None, 'tp'), may hold values from -0.125 to 0.125
- w_down: bfloat16 [8, 4096, 2048], P('sp', 'tp'), may hold values from -0.09375 to 0.09375
Outputs:
- layer_out: bfloat16 [2048, 2048], P(('sp', 'tp'))
Inputs may be any that keep to these rules, and one draw needn't show every extreme that they name: `expert_ids`: in each aligned block of 256 positions no expert is named by more than 80 routes, a bound that some block reaches; a token's experts differ. `cum_gates`: never rises along the positions.
All inputs are finite; a program needn't handle non-finite values.
Results may differ from a plain program's by a relative error of at most 0.015.
Values may be sent and summed in bfloat16 or wider, within the bound.
A program may use at most 64 MiB of HBM per device.

v0:
```python
import jax
import jax.numpy as jnp
from jax import lax
from jax.sharding import PartitionSpec as P

eps_norm = 1e-06
big_neg = -1e30


def rms_scale(values, gain):
    return values * lax.rsqrt(jnp.mean(values * values, axis=-1, keepdims=True) + eps_norm) * gain


def empty_state(item_count, heads, width):
    return (
        jnp.full((heads, item_count), big_neg, jnp.float32),
        jnp.zeros((heads, item_count), jnp.float32),
        jnp.zeros((heads, item_count, width), jnp.float32),
    )


def update_state(state, query, key_rows, values, query_gate, key_gate, mask, width):
    highest, total, accum = state
    score = jnp.einsum(
        "rhd,khd->hrk", query, key_rows, preferred_element_type=jnp.float32
    ) * width ** (-0.5)
    score = score + query_gate.T[:, :, None] - key_gate.T[:, None, :]
    new_high = jnp.maximum(highest, jnp.max(jnp.where(mask[None], score, big_neg), axis=2))
    expo = jnp.exp(jnp.where(mask[None], score - new_high[:, :, None], big_neg))
    total = jnp.sum(expo, axis=2)
    accum = jnp.einsum(
        "hrk,khd->hrd", expo.astype(jnp.bfloat16), values, preferred_element_type=jnp.float32
    )
    return (new_high, total, accum)


def finish(state):
    highest, total, accum = state
    heads, item_count, width = accum.shape
    result = accum / total[:, :, None]
    return result.transpose(1, 0, 2).reshape(item_count, heads * width).astype(jnp.bfloat16)


def per_device(
    residual_in,
    query_a,
    key_a,
    value_a,
    query_b,
    key_b,
    value_b,
    cum_gates,
    out_a,
    out_b,
    post_gain,
    pre_gain,
    expert_ids,
    expert_weights,
    w_gate,
    w_up,
    w_down,
):
    rows = query_a.shape[0]
    heads = cum_gates.shape[2]
    width_a = query_a.shape[1] // heads
    width_b = query_b.shape[1] // heads
    group_size = lax.axis_size("sp")
    narrow = lax.axis_size("tp")
    here = lax.axis_index("sp")
    offset = here * rows
    gates_all = lax.all_gather(cum_gates, "sp", axis=0, tiled=True)
    queries_a = query_a.reshape(rows, heads, width_a)
    queries_b = query_b.reshape(rows, heads, width_b)
    blocks = [(queries_a, queries_b, offset + jnp.arange(rows, dtype=jnp.int32), cum_gates)]
    initial = tuple(
        (
            (
                empty_state(block[2].shape[0], heads, width_a),
                empty_state(block[2].shape[0], heads, width_b),
            )
            for block in blocks
        )
    )
    start = jnp.int32(0)
    piece_key_a = lax.all_gather(key_a.reshape(rows, heads, width_a), "sp", axis=0, tiled=True)
    piece_value_a = lax.all_gather(value_a.reshape(rows, heads, width_a), "sp", axis=0, tiled=True)
    piece_key_b = lax.all_gather(key_b.reshape(rows, heads, width_b), "sp", axis=0, tiled=True)
    piece_value_b = lax.all_gather(value_b.reshape(rows, heads, width_b), "sp", axis=0, tiled=True)
    item_count = piece_key_a.shape[0]
    key_pos = jnp.arange(item_count, dtype=jnp.int32)
    updated = []
    for state, (block_a, block_b, position, block_gate) in zip(initial, blocks):

        def compute(current):
            mask = key_pos[None, :] <= position[:, None]
            return (
                update_state(
                    current[0],
                    block_a,
                    piece_key_a,
                    piece_value_a,
                    block_gate[:, 0, :],
                    gates_all[:, 0, :],
                    mask,
                    width_a,
                ),
                update_state(
                    current[1],
                    block_b,
                    piece_key_b,
                    piece_value_b,
                    block_gate[:, 1, :],
                    gates_all[:, 1, :],
                    mask,
                    width_b,
                ),
            )

        updated.append(lax.cond(start <= position[-1], compute, lambda current: current, state))
    folded = tuple(updated)
    attn_a = finish(folded[0][0])
    attn_b = finish(folded[0][1])
    proj = lax.psum_scatter(
        (
            jnp.dot(attn_a, out_a, preferred_element_type=jnp.float32)
            + jnp.dot(attn_b, out_b, preferred_element_type=jnp.float32)
        ).astype(jnp.bfloat16),
        "tp",
        scatter_dimension=0,
        tiled=True,
    )
    post = rms_scale(proj.astype(jnp.float32), post_gain.astype(jnp.float32))
    mid_stream = (residual_in.astype(jnp.float32) + post).astype(jnp.bfloat16)
    normed = rms_scale(mid_stream.astype(jnp.float32), pre_gain.astype(jnp.float32)).astype(
        jnp.bfloat16
    )
    selected_count = expert_ids.shape[1]
    columns = normed.shape[1] // narrow
    slots = rows * selected_count * 5 // (4 * group_size)
    flat_experts = expert_ids.reshape(-1)
    onehot = (flat_experts[:, None] == jnp.arange(group_size, dtype=jnp.int32)[None, :]).astype(
        jnp.int32
    )
    rank = jnp.sum((jnp.cumsum(onehot, axis=0) - onehot) * onehot, axis=1)
    target = flat_experts * slots + rank
    owner = jnp.arange(rows * selected_count, dtype=jnp.int32) // selected_count
    table = jnp.full((group_size * slots,), -1, jnp.int32).at[target].set(owner)
    live = table >= 0
    source = jnp.maximum(table, 0)
    weighting = jnp.sum(
        expert_weights[:, :, None]
        * (
            target.reshape(rows, selected_count)[:, :, None]
            == jnp.arange(group_size * slots, dtype=jnp.int32)[None, None, :]
        ),
        axis=1,
    )
    column_rows = lax.all_to_all(normed, "tp", split_axis=1, concat_axis=0, tiled=True)
    outgoing = jnp.where(live[:, None], column_rows[source], jnp.zeros((), jnp.bfloat16))
    outgoing = outgoing.reshape(group_size, slots, columns)
    arrived = lax.all_to_all(outgoing, "sp", split_axis=0, concat_axis=0, tiled=True)
    flat = arrived.reshape(-1, columns)
    piece = lax.all_gather(flat, "tp", axis=1, tiled=True)
    gate_rows = w_gate[0]
    up_rows = w_up[0]
    gate = jnp.dot(piece, gate_rows, preferred_element_type=jnp.float32)
    upward = jnp.dot(piece, up_rows, preferred_element_type=jnp.float32)
    hidden_rows = (jax.nn.silu(gate) * upward).astype(jnp.bfloat16)
    hidden = hidden_rows.reshape(arrived.shape[0], arrived.shape[1], -1)
    flat_hidden = hidden.reshape(-1, hidden.shape[2])
    down_cols = w_down[0]
    summed = lax.psum_scatter(
        lax.dot_general(
            down_cols, flat_hidden, (((0,), (1,)), ((), ())), preferred_element_type=jnp.float32
        ).astype(jnp.bfloat16),
        "tp",
        scatter_dimension=0,
        tiled=True,
    )
    returned = lax.all_to_all(
        summed.reshape(columns, group_size, slots), "sp", split_axis=1, concat_axis=1, tiled=True
    )
    mixture_cols = jnp.einsum(
        "te,ce->tc",
        weighting,
        returned.reshape(columns, group_size * slots).astype(jnp.float32),
        precision=lax.Precision.HIGHEST,
    )
    mixture = lax.all_to_all(
        mixture_cols.astype(jnp.bfloat16), "tp", split_axis=0, concat_axis=1, tiled=True
    ).astype(mixture_cols.dtype)
    return (mid_stream.astype(jnp.float32) + mixture).astype(jnp.bfloat16)


def solution(mesh):
    placed = (
        P(("sp", "tp"), None),
        P("sp", "tp"),
        P("sp", "tp"),
        P("sp", "tp"),
        P("sp", "tp"),
        P("sp", "tp"),
        P("sp", "tp"),
        P("sp", None, "tp"),
        P("tp", None),
        P("tp", None),
        P(),
        P(),
        P("sp", None),
        P("sp", None),
        P("sp", None, "tp"),
        P("sp", None, "tp"),
        P("sp", "tp", None),
    )
    return jax.shard_map(
        per_device, mesh=mesh, in_specs=placed, out_specs=P(("sp", "tp"), None), check_vma=False
    )
```

profile of v0, /device:TPU:0, one launch (start us, length us, event | category | flops | bytes accessed | tf_op | source)
XLA Modules:
  0.0 352.2 jit_solution(581141033529459929)
XLA Ops:
  6.5 1.8 copy.59
  8.3 0.0 all-gather.6.cloned.1.call-update
  8.4 0.0 all-gather.8.cloned.1.call-start
  8.4 1.7 copy.60
  10.1 0.0 all-gather.8.cloned.1.call-update
  10.1 0.0 all-gather.10.cloned.1.call-start
  10.2 1.8 copy.61
  11.9 0.0 all-gather.10.cloned.1.call-update
  12.0 0.0 all-gather.12.cloned.1.call-start
  12.0 1.8 copy.62
  13.8 0.0 all-gather.12.cloned.1.call-update
  13.8 0.0 reduce-scatter.3.cloned.1.call-start
  13.9 0.6 slice.21
  15.0 16.0 %all_gather.19 = f32[2048,2,4]{0,2,1:T(4,128)S(1)} all-gather(f32[256,2,4]{0,2,1:T(4,128)} %param.26), channel_id=1, replica_groups=mesh['sp'=8,'tp'=4] {'sp'}, dimensions={0}, use_global_device_ids=true | all-gather | bytes 73728 | tf_op jit(solution)/shard_map/all_gather | solution.py:71
  31.0 4.8 %all-gather.6.cloned.1.call-done = bf16[2048,4,64]{0,2,1:T(8,128)(2,1)} async-done(((bf16[256,4,64]{0,2,1:T(8,128)(2,1)}), bf16[2048,4,64]{0,2,1:T(8,128)(2,1)}) %all-gather.6.cloned.1.call-update) | async-done | bytes 1048592 | tf_op jit(solution)/shard_map/all_gather | solution.py:85
  35.9 25.3 %all-gather.8.cloned.1.call-done = bf16[2048,4,64]{0,2,1:T(8,128)(2,1)} async-done(((bf16[256,4,64]{0,2,1:T(8,128)(2,1)}), bf16[2048,4,64]{0,2,1:T(8,128)(2,1)}) %all-gather.8.cloned.1.call-update) | async-done | bytes 1048592 | tf_op jit(solution)/shard_map/all_gather | solution.py:86
  61.2 31.0 %all-gather.10.cloned.1.call-done = bf16[2048,4,128]{0,2,1:T(8,128)(2,1)} async-done(((bf16[256,4,128]{0,2,1:T(8,128)(2,1)}), bf16[2048,4,128]{0,2,1:T(8,128)(2,1)}) %all-gather.10.cloned.1.call-update) | async-done | bytes 2097168 | tf_op jit(solution)/shard_map/all_gather | solution.py:87
  92.2 31.1 %all-gather.12.cloned.1.call-done = bf16[2048,4,128]{0,2,1:T(8,128)(2,1)} async-done(((bf16[256,4,128]{0,2,1:T(8,128)(2,1)}), bf16[2048,4,128]{0,2,1:T(8,128)(2,1)}) %all-gather.12.cloned.1.call-update) | async-done | bytes 2097168 | tf_op jit(solution)/shard_map/all_gather | solution.py:88
  123.3 22.6 %conditional.1 = (f32[4,256]{1,0:T(4,128)S(1)}, f32[4,256,64]{1,2,0:T(8,128)S(1)}, f32[4,256]{1,0:T(4,128)S(1)}, f32[4,256,128]{1,2,0:T(8,128)S(1)}) conditional(s32[]{:T(128)} %bitcast.9, () %tuple.13, (s32[2048]{0:T(1024)S(1)}, s32[256]{0:T(256)S(1)}, bf16[256,256]{1,0:T(8,128)(2,1)}, bf16[2048,4,64]{0,2,1:T(8,128)(2,1)}, f32[256,2,4]{0,2,1:T(4,128)}, ...), branch_computations={%region_0.0_spmd, %region_1.6_spmd} | conditional | flops 1682438144 | bytes 83133552 | solution.py:119
  123.3 0.7 slice_bitcast_fusion.3
  124.0 1.0 copy.63
  125.1 0.4 broadcast_compare_fusion
  125.4 2.7 fusion.53
  128.2 4.5 %select_reduce_fusion = (f32[4,256]{1,0:T(4,128)S(1)}, f32[4,256]{1,0:T(4,128)S(1)}, f32[4,256,2048]{2,1,0:T(8,128)S(1)}) fusion(f32[4,2048]{1,0:T(4,128)S(1)} %get-tuple-element.97, f32[4,256]{1,0:T(4,128)S(1)} %get-tuple-element.99, pred[256,2048]{1,0:T(8,128)(4,1)S(1)} %broadcast_compare_fusion, f32[4,2048]{1,0:T(4,128)S(1)} %get-tuple-element.96, ...), kind=kOutput, calls=%fused_computation.3 | convolution fusion | flops 557840384 | bytes 19742720 | tf_op jit(solution)/shard_map/cond/branch_1_fun/rhd,khd->hrk/dot_general | solution.py:24
  132.7 2.8 fusion.6
  135.5 5.9 %fusion.3 = (f32[4,256]{1,0:T(4,128)S(1)}, f32[4,256]{1,0:T(4,128)S(1)}) fusion(f32[4,256,2048]{2,1,0:T(8,128)S(1)} %get-tuple-element.100, f32[4,256]{1,0:T(4,128)S(1)} %get-tuple-element.101, f32[4,2048]{1,0:T(4,128)S(1)} %get-tuple-element.97, f32[4,256]{1,0:T(4,128)S(1)} %get-tuple-element.99, pred[256,2048]{1,0:T(8,128)(4,1)S(1)} %broadcast_compare_fusion, ...), kind=kLoop, calls=%fused_computation.11 | loop fusion | flops 25163776 | bytes 17391616 | tf_op jit(solution)/shard_map/cond/branch_1_fun/reduce_sum | solution.py:30
  141.4 4.3 %fusion.4 = f32[4,256,128]{1,2,0:T(8,128)S(1)} fusion(bf16[2048,4,128]{0,2,1:T(8,128)(2,1)} %get-tuple-element.88, f32[4,256,2048]{2,1,0:T(8,128)S(1)} %get-tuple-element.100, f32[4,256]{1,0:T(4,128)S(1)} %get-tuple-element.101, f32[4,2048]{1,0:T(4,128)S(1)} %get-tuple-element.97, f32[4,256]{1,0:T(4,128)S(1)} %get-tuple-element.99, ...), kind=kOutput, calls=%fused_computation.12 | convolution fusion | flops 549453824 | bytes 11575296 | tf_op jit(solution)/shard_map/cond | solution.py:119
  146.0 1.7 fusion.54
  147.8 1.7 fusion.29
  149.5 0.1 copy.67
  149.7 0.1 eq.42
  149.8 0.1 eq.38
  150.0 1.1 reduce-window.6
  151.1 0.2 slice_reduce_fusion
  151.4 0.1 fusion.43
  151.5 0.1 reduce_sum.60
  151.7 0.1 mul.94
  151.8 2.4 scatter_custom_fusion
  154.3 22.3 %reduce-scatter.3.cloned.1.call-done = bf16[64,2048]{1,0:T(8,128)(2,1)} async-done(((bf16[256,2048]{1,0:T(8,128)(2,1)}), bf16[64,2048]{1,0:T(8,128)(2,1)}) %reduce-scatter.3.cloned.1.call-update) | async-done | bytes 262160 | tf_op jit(solution)/shard_map/reduce_scatter | solution.py:123
  176.6 1.1 fusion.34
  177.8 1.3 fusion.38
  179.0 0.7 copy-done.1
  179.7 0.1 fusion.40
  179.9 0.7 copy.87
  180.6 3.4 all-to-all-start
  184.0 0.0 all-gather.14.cloned.1.call-start
  184.1 0.1 broadcast_in_dim.74
  184.2 5.3 %all-to-all-done = bf16[64,4,512]{2,0,1:T(8,128)(2,1)S(1)} async-done(((bf16[64,4,512]{2,0,1:T(8,128)(2,1)}), bf16[64,4,512]{2,0,1:T(8,128)(2,1)S(1)}, u32[]{:S(2)}, u32[]{:S(2)}) %all-to-all-start) | async-done | bytes 262176 | tf_op jit(solution)/shard_map/all_to_all | solution.py:158
  189.5 2.8 gather_fusion
  192.2 0.2 broadcast_select_fusion
  192.4 22.6 %all_to_all.42 = bf16[8,80,512]{2,1,0:T(8,128)(2,1)} all-to-all(bf16[8,80,512]{2,1,0:T(8,128)(2,1)S(1)} %broadcast_select_fusion), channel_id=1, replica_groups=mesh['sp'=8,'tp'=4] {'sp'}, dimensions={0} | all-to-all | bytes 1310720 | tf_op jit(solution)/shard_map/all_to_all | solution.py:161
  215.0 0.0 all-gather.14.cloned.1.call-update
  215.1 0.0 reduce-scatter.5.cloned.1.call-start
  215.1 37.2 %all-gather.14.cloned.1.call-done = bf16[640,2048]{1,0:T(8,128)(2,1)} async-done(((bf16[640,512]{1,0:T(8,128)(2,1)}), bf16[640,2048]{1,0:T(8,128)(2,1)}) %all-gather.14.cloned.1.call-update) | async-done | bytes 2621456 | tf_op jit(solution)/shard_map/all_gather | solution.py:163
  252.4 7.4 %fusion.19 = f32[640,1024]{1,0:T(8,128)} fusion(bf16[640,2048]{1,0:T(8,128)(2,1)} %all-gather.14.cloned.1.call-done, bf16[1,2048,1024]{2,1,0:T(8,128)(2,1)} %param.34), kind=kOutput, calls=%fused_computation.32 | convolution fusion | flops 2684354560 | bytes 9437184 | tf_op jit(solution)/shard_map/dot_general | solution.py:167
  259.7 12.3 %fusion.26 = bf16[2048,640]{0,1:T(8,128)(2,1)} fusion(bf16[1,1024,2048]{2,1,0:T(8,128)(2,1)} %param.35, f32[640,1024]{1,0:T(8,128)} %fusion.19, bf16[640,2048]{1,0:T(8,128)(2,1)} %all-gather.14.cloned.1.call-done, bf16[1,2048,1024]{2,1,0:T(8,128)(2,1)} %param.33), kind=kOutput, calls=%fused_computation.37 | convolution fusion | flops 5373952000 | bytes 16252928 | tf_op jit(solution)/shard_map/dot_general | solution.py:173
  272.0 39.7 %reduce-scatter.5.cloned.1.call-done = bf16[512,640]{0,1:T(8,128)(2,1)} async-done(((bf16[2048,640]{0,1:T(8,128)(2,1)}), bf16[512,640]{0,1:T(8,128)(2,1)}) %reduce-scatter.5.cloned.1.call-update) | async-done | bytes 655376 | tf_op jit(solution)/shard_map/reduce_scatter | solution.py:172
  311.8 4.6 %all-to-all-start.2 = ((bf16[512,8,80]{0,2,1:T(8,128)(2,1)}), bf16[512,8,80]{0,2,1:T(8,128)(2,1)S(1)}, u32[]{:S(2)}, u32[]{:S(2)}) async-start(bf16[512,8,80]{0,2,1:T(8,128)(2,1)} %bitcast.106), calls=%async_computation.4 | async-start | bytes 1310720 | tf_op jit(solution)/shard_map/all_to_all | solution.py:180
  316.3 0.1 copy.70
  316.4 0.2 select_reduce_fusion.2
  316.7 17.8 %all-to-all-done.2 = bf16[512,8,80]{0,2,1:T(8,128)(2,1)S(1)} async-done(((bf16[512,8,80]{0,2,1:T(8,128)(2,1)}), bf16[512,8,80]{0,2,1:T(8,128)(2,1)S(1)}, u32[]{:S(2)}, u32[]{:S(2)}) %all-to-all-start.2) | async-done | bytes 655392 | tf_op jit(solution)/shard_map/all_to_all | solution.py:180
  334.5 0.8 convolution_convert_fusion
  335.3 8.3 %all_to_all.43 = bf16[4,64,512]{2,1,0:T(8,128)(2,1)S(1)} all-to-all(bf16[4,64,512]{2,1,0:T(8,128)(2,1)S(1)} %bitcast.104), channel_id=1, replica_groups=mesh['sp'=8,'tp'=4] {'tp'}, dimensions={0} | all-to-all | bytes 524288 | tf_op jit(solution)/shard_map/all_to_all | solution.py:189
  343.7 1.7 fusion.41
  (43 shorter events, 0.4 us)
Async XLA Ops:
  6.5 141.2 %copy-start = (bf16[512,2048]{1,0:T(8,128)(2,1)S(1)}, bf16[512,2048]{1,0:T(8,128)(2,1)}, u32[]{:S(2)}) copy-start(bf16[512,2048]{1,0:T(8,128)(2,1)} %param.28) | copy-start | bytes 6291460
  6.5 29.3 %all-gather.6.cloned.1.call-start = ((), (), s32[]{:S(2)}) async-start(), calls=%async_computation.6 | async-start | bytes 1179648 | tf_op jit(solution)/shard_map/all_gather | solution.py:85
  8.4 52.8 %all-gather.8.cloned.1.call-start = ((), (), s32[]{:S(2)}) async-start(), calls=%async_computation.7 | async-start | bytes 1179648 | tf_op jit(solution)/shard_map/all_gather | solution.py:86
  10.1 82.1 %all-gather.10.cloned.1.call-start = ((), (), s32[]{:S(2)}) async-start(), calls=%async_computation.8 | async-start | bytes 2359296 | tf_op jit(solution)/shard_map/all_gather | solution.py:87
  12.0 111.3 %all-gather.12.cloned.1.call-start = ((), (), s32[]{:S(2)}) async-start(), calls=%async_computation.9 | async-start | bytes 2359296 | tf_op jit(solution)/shard_map/all_gather | solution.py:88
  13.8 162.8 %reduce-scatter.3.cloned.1.call-start = ((), (), s32[]{:S(2)}) async-start(), calls=%async_computation.10 | async-start | bytes 1310720 | tf_op jit(solution)/shard_map/reduce_scatter | solution.py:123
  124.0 4.1 %copy-start.9 = (bf16[256,512]{1,0:T(8,128)(2,1)S(1)}, bf16[256,512]{1,0:T(8,128)(2,1)}, u32[]{:S(2)}) copy-start(bf16[256,512]{1,0:T(8,128)(2,1)} %get-tuple-element.48) | copy-start | bytes 786436 | tf_op jit(solution)/shard_map/cond
  125.1 3.1 copy-start.7
  128.2 4.5 %copy-start.8 = (bf16[2048,4,64]{0,2,1:T(8,128)(2,1)S(1)}, bf16[2048,4,64]{0,2,1:T(8,128)(2,1)}, u32[]{:S(2)}) copy-start(bf16[2048,4,64]{0,2,1:T(8,128)(2,1)} %get-tuple-element.33) | copy-start | bytes 3145732 | tf_op jit(solution)/shard_map/cond
  145.9 3.6 %copy-start.5 = (s32[256,2]{0,1:T(2,128)S(1)}, s32[256,2]{0,1:T(2,128)}, u32[]{:S(2)}) copy-start(s32[256,2]{0,1:T(2,128)} %param.31) | copy-start | bytes 6148
  146.0 4.0 %copy-start.3 = (bf16[2048]{0:T(1024)(128)(2,1)S(1)}, bf16[2048]{0:T(1024)(128)(2,1)}, u32[]{:S(2)}) copy-start(bf16[2048]{0:T(1024)(128)(2,1)} %param.29) | copy-start | bytes 12292
  146.0 4.0 %copy-start.4 = (bf16[2048]{0:T(1024)(128)(2,1)S(1)}, bf16[2048]{0:T(1024)(128)(2,1)}, u32[]{:S(2)}) copy-start(bf16[2048]{0:T(1024)(128)(2,1)} %param.30) | copy-start | bytes 12292
  146.0 31.7 %copy-start.2 = (bf16[64,2048]{1,0:T(8,128)(2,1)S(1)}, bf16[64,2048]{1,0:T(8,128)(2,1)}, u32[]{:S(2)}) copy-start(bf16[64,2048]{1,0:T(8,128)(2,1)} %param.19) | copy-start | bytes 786436
  179.0 0.7 copy-start.1
  180.6 8.9 %all-to-all-start = ((bf16[64,4,512]{2,0,1:T(8,128)(2,1)}), bf16[64,4,512]{2,0,1:T(8,128)(2,1)S(1)}, u32[]{:S(2)}, u32[]{:S(2)}) async-start(bf16[64,4,512]{2,0,1:T(8,128)(2,1)} %bitcast.94), calls=%async_computation.1 | async-start | bytes 524288 | tf_op jit(solution)/shard_map/all_to_all | solution.py:158
  184.0 68.3 %all-gather.14.cloned.1.call-start = ((), (), s32[]{:S(2)}) async-start(), calls=%async_computation.11 | async-start | bytes 3276800 | tf_op jit(solution)/shard_map/all_gather | solution.py:163
  215.1 96.7 %reduce-scatter.5.cloned.1.call-start = ((), (), s32[]{:S(2)}) async-start(), calls=%async_computation.12 | async-start | bytes 3276800 | tf_op jit(solution)/shard_map/reduce_scatter | solution.py:172
  259.7 56.7 %copy-start.6 = (f32[256,2]{0,1:T(2,128)S(1)}, f32[256,2]{0,1:T(2,128)}, u32[]{:S(2)}) copy-start(f32[256,2]{0,1:T(2,128)} %param.32) | copy-start | bytes 6148
  311.8 22.7 %all-to-all-start.2 = ((bf16[512,8,80]{0,2,1:T(8,128)(2,1)}), bf16[512,8,80]{0,2,1:T(8,128)(2,1)S(1)}, u32[]{:S(2)}, u32[]{:S(2)}) async-start(bf16[512,8,80]{0,2,1:T(8,128)(2,1)} %bitcast.106), calls=%async_computation.4 | async-start | bytes 1310720 | tf_op jit(solution)/shard_map/all_to_all | solution.py:180
Sparse Core Ops, SparseCore 0:
  8.9 26.9 all-gather.5
  37.5 23.6 all-gather.7
  62.8 29.3 all-gather.9
  93.6 29.6 all-gather.11
  149.6 26.9 reduce-scatter.2
  215.2 37.1 all-gather.13
  272.2 39.5 reduce-scatter.4
where the time goes:
time: 353 us; the launch traced here: 352 us
  waiting for transfers between devices  215 us (61%)
  blocking collectives  46.9 us (13%)
  matrix products  38.2 us (11%)
  local copies, waits for them, and re-layouts  17.2 us (5%)
  between operations  14.4 us (4%)
  other arithmetic  12.3 us (3%)
  starting transfers between devices  8.24 us (2%)
    reduce_scatter x1, waiting for transfers between devices, per_device(): lax.psum_scatter(lax.dot_general(down_cols, flat_hidden, (((0,), (1,)), (...  39.7 us
    all_gather x1, waiting for transfers between devices, per_device(): piece = lax.all_gather(flat, 'tp', axis=1, tiled=True)  37.2 us
    all_gather x1, waiting for transfers between devices, per_device(): lax.all_gather(value_b.reshape(rows, heads, width_b), 'sp', axis=0, tiled...  31.1 us
    all_gather x1, waiting for transfers between devices, per_device(): lax.all_gather(key_b.reshape(rows, heads, width_b), 'sp', axis=0, tiled=T...  31 us
    all_gather x1, waiting for transfers between devices, per_device(): lax.all_gather(value_a.reshape(rows, heads, width_a), 'sp', axis=0, tiled...  25.3 us
    all_to_all x1, blocking collectives, per_device(): lax.all_to_all(outgoing, 'sp', split_axis=0, concat_axis=0, tiled=True)  22.6 us
    reduce_scatter x1, waiting for transfers between devices, per_device(): lax.psum_scatter((jnp.dot(attn_a, out_a, preferred_element_type=jnp.float...  22.3 us
    all_to_all x1, waiting for transfers between devices, per_device(): lax.all_to_all(summed.reshape(columns, group_size, slots), 'sp', split_ax...  17.8 us
  transfers between devices with their start and end apart: 9, of which 9 were waited for; matrix products, arithmetic and copies ran while one was open for 3% of the time, Pallas kernels for 0%

commit v1 on v0

--- a/solution.py
+++ b/solution.py
@@ -5,6 +5,19 @@
 
 eps_norm = 1e-06
 big_neg = -1e30
+
+
+def handle_ends(inner_x):
+    clean = jnp.concatenate(
+        lax.all_to_all(
+            jnp.stack(jnp.split(inner_x, lax.axis_size("sp"), axis=1)),
+            axis_name="sp",
+            split_axis=0,
+            concat_axis=0,
+        ),
+        axis=1,
+    )
+    return clean
 
 
 def rms_scale(values, gain):
@@ -177,9 +190,7 @@
         scatter_dimension=0,
         tiled=True,
     )
-    returned = lax.all_to_all(
-        summed.reshape(columns, group_size, slots), "sp", split_axis=1, concat_axis=1, tiled=True
-    )
+    returned = handle_ends(summed.reshape(columns, group_size, slots))
     mixture_cols = jnp.einsum(
         "te,ce->tc",
         weighting,

time: 353 us -> 365 us (1.034)
  local copies, waits for them, and re-layouts: 17.2 us -> 29.4 us
    unnamed x19 -> x26, local copies, waits for them, and re-layouts: 7.91 us -> 18.6 us
where the time goes in v1:
time: 365 us; the launch traced here: 364 us
  waiting for transfers between devices  215 us (59%)
  blocking collectives  46.9 us (13%)
  matrix products  38.2 us (10%)
  local copies, waits for them, and re-layouts  29.4 us (8%)
  between operations  14.4 us (4%)
  other arithmetic  12.3 us (3%)
  starting transfers between devices  8.26 us (2%)
    reduce_scatter x1, waiting for transfers between devices, per_device(): lax.psum_scatter(lax.dot_general(down_cols, flat_hidden, (((0,), (1,)), (...  39.7 us
    all_gather x1, waiting for transfers between devices, per_device(): piece = lax.all_gather(flat, 'tp', axis=1, tiled=True)  37.2 us
    all_gather x1, waiting for transfers between devices, per_device(): lax.all_gather(value_b.reshape(rows, heads, width_b), 'sp', axis=0, tiled...  31.1 us
    all_gather x1, waiting for transfers between devices, per_device(): lax.all_gather(key_b.reshape(rows, heads, width_b), 'sp', axis=0, tiled=T...  31 us
    all_gather x1, waiting for transfers between devices, per_device(): lax.all_gather(value_a.reshape(rows, heads, width_a), 'sp', axis=0, tiled...  25.3 us
    all_to_all x1, blocking collectives, per_device(): lax.all_to_all(outgoing, 'sp', split_axis=0, concat_axis=0, tiled=True)  22.6 us
    reduce_scatter x1, waiting for transfers between devices, per_device(): lax.psum_scatter((jnp.dot(attn_a, out_a, preferred_element_type=jnp.float...  22.3 us
    unnamed x26, local copies, waits for them, and re-layouts  18.6 us
  transfers between devices with their start and end apart: 9, of which 9 were waited for; matrix products, arithmetic and copies ran while one was open for 3% of the time, Pallas kernels for 0%

profile of v1, /device:TPU:0, one launch (start us, length us, event | category | flops | bytes accessed | tf_op | source)
XLA Modules:
  0.0 364.4 jit_solution(5493891955284571159)
XLA Ops:
  6.5 1.8 copy.59
  8.4 0.0 all-gather.8.cloned.1.call-start
  8.4 1.7 copy.60
  10.2 1.8 copy.61
  12.0 1.8 copy.62
  13.8 0.0 reduce-scatter.3.cloned.1.call-start
  13.9 0.6 slice.21
  15.0 16.0 %all_gather.19 = f32[2048,2,4]{0,2,1:T(4,128)S(1)} all-gather(f32[256,2,4]{0,2,1:T(4,128)} %param.26), channel_id=1, replica_groups=mesh['sp'=8,'tp'=4] {'sp'}, dimensions={0}, use_global_device_ids=true | all-gather | bytes 73728 | tf_op jit(solution)/shard_map/all_gather | solution.py:84
  31.0 4.8 %all-gather.6.cloned.1.call-done = bf16[2048,4,64]{0,2,1:T(8,128)(2,1)} async-done(((bf16[256,4,64]{0,2,1:T(8,128)(2,1)}), bf16[2048,4,64]{0,2,1:T(8,128)(2,1)}) %all-gather.6.cloned.1.call-update) | async-done | bytes 1048592 | tf_op jit(solution)/shard_map/all_gather | solution.py:98
  35.9 25.3 %all-gather.8.cloned.1.call-done = bf16[2048,4,64]{0,2,1:T(8,128)(2,1)} async-done(((bf16[256,4,64]{0,2,1:T(8,128)(2,1)}), bf16[2048,4,64]{0,2,1:T(8,128)(2,1)}) %all-gather.8.cloned.1.call-update) | async-done | bytes 1048592 | tf_op jit(solution)/shard_map/all_gather | solution.py:99
  61.2 31.0 %all-gather.10.cloned.1.call-done = bf16[2048,4,128]{0,2,1:T(8,128)(2,1)} async-done(((bf16[256,4,128]{0,2,1:T(8,128)(2,1)}), bf16[2048,4,128]{0,2,1:T(8,128)(2,1)}) %all-gather.10.cloned.1.call-update) | async-done | bytes 2097168 | tf_op jit(solution)/shard_map/all_gather | solution.py:100
  92.2 31.1 %all-gather.12.cloned.1.call-done = bf16[2048,4,128]{0,2,1:T(8,128)(2,1)} async-done(((bf16[256,4,128]{0,2,1:T(8,128)(2,1)}), bf16[2048,4,128]{0,2,1:T(8,128)(2,1)}) %all-gather.12.cloned.1.call-update) | async-done | bytes 2097168 | tf_op jit(solution)/shard_map/all_gather | solution.py:101
  123.3 22.6 %conditional.1 = (f32[4,256]{1,0:T(4,128)S(1)}, f32[4,256,64]{1,2,0:T(8,128)S(1)}, f32[4,256]{1,0:T(4,128)S(1)}, f32[4,256,128]{1,2,0:T(8,128)S(1)}) conditional(s32[]{:T(128)} %bitcast.9, () %tuple.13, (s32[2048]{0:T(1024)S(1)}, s32[256]{0:T(256)S(1)}, bf16[256,256]{1,0:T(8,128)(2,1)}, bf16[2048,4,64]{0,2,1:T(8,128)(2,1)}, f32[256,2,4]{0,2,1:T(4,128)}, ...), branch_computations={%region_0.0_spmd, %region_1.6_spmd} | conditional | flops 1682438144 | bytes 83133552 | solution.py:132
  123.3 0.7 slice_bitcast_fusion.3
  124.0 1.0 copy.63
  125.1 0.4 broadcast_compare_fusion
  125.4 2.7 fusion.61
  128.2 4.5 %select_reduce_fusion = (f32[4,256]{1,0:T(4,128)S(1)}, f32[4,256]{1,0:T(4,128)S(1)}, f32[4,256,2048]{2,1,0:T(8,128)S(1)}) fusion(f32[4,2048]{1,0:T(4,128)S(1)} %get-tuple-element.97, f32[4,256]{1,0:T(4,128)S(1)} %get-tuple-element.99, pred[256,2048]{1,0:T(8,128)(4,1)S(1)} %broadcast_compare_fusion, f32[4,2048]{1,0:T(4,128)S(1)} %get-tuple-element.96, ...), kind=kOutput, calls=%fused_computation.3 | convolution fusion | flops 557840384 | bytes 19742720 | tf_op jit(solution)/shard_map/cond/branch_1_fun/rhd,khd->hrk/dot_general | solution.py:37
  132.7 2.8 fusion.6
  135.5 5.9 %fusion.3 = (f32[4,256]{1,0:T(4,128)S(1)}, f32[4,256]{1,0:T(4,128)S(1)}) fusion(f32[4,256,2048]{2,1,0:T(8,128)S(1)} %get-tuple-element.100, f32[4,256]{1,0:T(4,128)S(1)} %get-tuple-element.101, f32[4,2048]{1,0:T(4,128)S(1)} %get-tuple-element.97, f32[4,256]{1,0:T(4,128)S(1)} %get-tuple-element.99, pred[256,2048]{1,0:T(8,128)(4,1)S(1)} %broadcast_compare_fusion, ...), kind=kLoop, calls=%fused_computation.11 | loop fusion | flops 25163776 | bytes 17391616 | tf_op jit(solution)/shard_map/cond/branch_1_fun/reduce_sum | solution.py:43
  141.4 4.3 %fusion.4 = f32[4,256,128]{1,2,0:T(8,128)S(1)} fusion(bf16[2048,4,128]{0,2,1:T(8,128)(2,1)} %get-tuple-element.88, f32[4,256,2048]{2,1,0:T(8,128)S(1)} %get-tuple-element.100, f32[4,256]{1,0:T(4,128)S(1)} %get-tuple-element.101, f32[4,2048]{1,0:T(4,128)S(1)} %get-tuple-element.97, f32[4,256]{1,0:T(4,128)S(1)} %get-tuple-element.99, ...), kind=kOutput, calls=%fused_computation.12 | convolution fusion | flops 549453824 | bytes 11575296 | tf_op jit(solution)/shard_map/cond | solution.py:132
  146.0 1.7 fusion.62
  147.8 1.7 fusion.29
  149.5 0.1 copy.67
  149.7 0.1 eq.42
  149.8 0.1 eq.38
  150.0 1.1 reduce-window.6
  151.1 0.2 slice_reduce_fusion
  151.4 0.1 fusion.51
  151.5 0.1 reduce_sum.60
  151.7 0.1 mul.94
  151.8 2.4 scatter_custom_fusion
  154.3 22.3 %reduce-scatter.3.cloned.1.call-done = bf16[64,2048]{1,0:T(8,128)(2,1)} async-done(((bf16[256,2048]{1,0:T(8,128)(2,1)}), bf16[64,2048]{1,0:T(8,128)(2,1)}) %reduce-scatter.3.cloned.1.call-update) | async-done | bytes 262160 | tf_op jit(solution)/shard_map/reduce_scatter | solution.py:136
  176.6 1.1 fusion.34
  177.8 1.3 fusion.38
  179.0 0.7 copy-done.1
  179.7 0.1 fusion.40
  179.9 0.7 copy.87
  180.6 3.4 all-to-all-start
  184.1 0.1 broadcast_in_dim.74
  184.2 5.3 %all-to-all-done = bf16[64,4,512]{2,0,1:T(8,128)(2,1)S(1)} async-done(((bf16[64,4,512]{2,0,1:T(8,128)(2,1)}), bf16[64,4,512]{2,0,1:T(8,128)(2,1)S(1)}, u32[]{:S(2)}, u32[]{:S(2)}) %all-to-all-start) | async-done | bytes 262176 | tf_op jit(solution)/shard_map/all_to_all | solution.py:171
  189.5 2.8 gather_fusion
  192.2 0.2 broadcast_select_fusion
  192.4 22.6 %all_to_all.42 = bf16[8,80,512]{2,1,0:T(8,128)(2,1)} all-to-all(bf16[8,80,512]{2,1,0:T(8,128)(2,1)S(1)} %broadcast_select_fusion), channel_id=1, replica_groups=mesh['sp'=8,'tp'=4] {'sp'}, dimensions={0} | all-to-all | bytes 1310720 | tf_op jit(solution)/shard_map/all_to_all | solution.py:174
  215.1 0.0 reduce-scatter.5.cloned.1.call-start
  215.1 37.2 %all-gather.14.cloned.1.call-done = bf16[640,2048]{1,0:T(8,128)(2,1)} async-done(((bf16[640,512]{1,0:T(8,128)(2,1)}), bf16[640,2048]{1,0:T(8,128)(2,1)}) %all-gather.14.cloned.1.call-update) | async-done | bytes 2621456 | tf_op jit(solution)/shard_map/all_gather | solution.py:176
  252.4 7.4 %fusion.19 = f32[640,1024]{1,0:T(8,128)} fusion(bf16[640,2048]{1,0:T(8,128)(2,1)} %all-gather.14.cloned.1.call-done, bf16[1,2048,1024]{2,1,0:T(8,128)(2,1)} %param.34), kind=kOutput, calls=%fused_computation.32 | convolution fusion | flops 2684354560 | bytes 9437184 | tf_op jit(solution)/shard_map/dot_general | solution.py:180
  259.7 12.3 %fusion.26 = bf16[2048,640]{0,1:T(8,128)(2,1)} fusion(bf16[1,1024,2048]{2,1,0:T(8,128)(2,1)} %param.35, f32[640,1024]{1,0:T(8,128)} %fusion.19, bf16[640,2048]{1,0:T(8,128)(2,1)} %all-gather.14.cloned.1.call-done, bf16[1,2048,1024]{2,1,0:T(8,128)(2,1)} %param.33), kind=kOutput, calls=%fused_computation.37 | convolution fusion | flops 5373952000 | bytes 16252928 | tf_op jit(solution)/shard_map/dot_general | solution.py:186
  272.0 39.7 %reduce-scatter.5.cloned.1.call-done = bf16[512,640]{0,1:T(8,128)(2,1)} async-done(((bf16[2048,640]{0,1:T(8,128)(2,1)}), bf16[512,640]{0,1:T(8,128)(2,1)}) %reduce-scatter.5.cloned.1.call-update) | async-done | bytes 655376 | tf_op jit(solution)/shard_map/reduce_scatter | solution.py:185
  311.8 1.5 fusion.49
  313.3 1.5 fusion.48
  314.8 1.5 fusion.47
  316.3 1.5 fusion.46
  317.9 1.5 fusion.45
  319.4 1.5 fusion.44
  320.9 1.5 fusion.43
  322.4 1.5 fusion.42
  323.9 4.6 %all-to-all-start.2 = ((bf16[8,512,1,80]{1,3,2,0:T(8,128)(2,1)}), bf16[8,512,1,80]{1,3,2,0:T(8,128)(2,1)S(1)}, u32[]{:S(2)}, u32[]{:S(2)}) async-start(bf16[8,512,1,80]{1,3,2,0:T(8,128)(2,1)} %fusion.42), calls=%async_computation.4 | async-start | bytes 1310720 | tf_op jit(solution)/shard_map/all_to_all | solution.py:12
  328.6 0.1 copy.70
  328.6 0.2 select_reduce_fusion.2
  328.9 17.8 %all-to-all-done.2 = bf16[8,512,1,80]{1,3,2,0:T(8,128)(2,1)S(1)} async-done(((bf16[8,512,1,80]{1,3,2,0:T(8,128)(2,1)}), bf16[8,512,1,80]{1,3,2,0:T(8,128)(2,1)S(1)}, u32[]{:S(2)}, u32[]{:S(2)}) %all-to-all-start.2) | async-done | bytes 655392 | tf_op jit(solution)/shard_map/all_to_all | solution.py:12
  346.7 0.8 convolution_convert_fusion
  347.5 8.3 %all_to_all.43 = bf16[4,64,512]{2,1,0:T(8,128)(2,1)S(1)} all-to-all(bf16[4,64,512]{2,1,0:T(8,128)(2,1)S(1)} %bitcast.138), channel_id=1, replica_groups=mesh['sp'=8,'tp'=4] {'tp'}, dimensions={0} | all-to-all | bytes 524288 | tf_op jit(solution)/shard_map/all_to_all | solution.py:200
  355.8 1.7 fusion.41
  (51 shorter events, 0.6 us)
Async XLA Ops:
  6.5 141.2 %copy-start = (bf16[512,2048]{1,0:T(8,128)(2,1)S(1)}, bf16[512,2048]{1,0:T(8,128)(2,1)}, u32[]{:S(2)}) copy-start(bf16[512,2048]{1,0:T(8,128)(2,1)} %param.28) | copy-start | bytes 6291460
  6.5 29.3 %all-gather.6.cloned.1.call-start = ((), (), s32[]{:S(2)}) async-start(), calls=%async_computation.6 | async-start | bytes 1179648 | tf_op jit(solution)/shard_map/all_gather | solution.py:98
  8.4 52.8 %all-gather.8.cloned.1.call-start = ((), (), s32[]{:S(2)}) async-start(), calls=%async_computation.7 | async-start | bytes 1179648 | tf_op jit(solution)/shard_map/all_gather | solution.py:99
  10.1 82.1 %all-gather.10.cloned.1.call-start = ((), (), s32[]{:S(2)}) async-start(), calls=%async_computation.8 | async-start | bytes 2359296 | tf_op jit(solution)/shard_map/all_gather | solution.py:100
  12.0 111.3 %all-gather.12.cloned.1.call-start = ((), (), s32[]{:S(2)}) async-start(), calls=%async_computation.9 | async-start | bytes 2359296 | tf_op jit(solution)/shard_map/all_gather | solution.py:101
  13.8 162.8 %reduce-scatter.3.cloned.1.call-start = ((), (), s32[]{:S(2)}) async-start(), calls=%async_computation.10 | async-start | bytes 1310720 | tf_op jit(solution)/shard_map/reduce_scatter | solution.py:136
  124.0 4.1 %copy-start.9 = (bf16[256,512]{1,0:T(8,128)(2,1)S(1)}, bf16[256,512]{1,0:T(8,128)(2,1)}, u32[]{:S(2)}) copy-start(bf16[256,512]{1,0:T(8,128)(2,1)} %get-tuple-element.48) | copy-start | bytes 786436 | tf_op jit(solution)/shard_map/cond
  125.1 3.1 copy-start.7
  128.2 4.5 %copy-start.8 = (bf16[2048,4,64]{0,2,1:T(8,128)(2,1)S(1)}, bf16[2048,4,64]{0,2,1:T(8,128)(2,1)}, u32[]{:S(2)}) copy-start(bf16[2048,4,64]{0,2,1:T(8,128)(2,1)} %get-tuple-element.33) | copy-start | bytes 3145732 | tf_op jit(solution)/shard_map/cond
  145.9 3.6 copy-start.5
  146.0 4.0 %copy-start.3 = (bf16[2048]{0:T(1024)(128)(2,1)S(1)}, bf16[2048]{0:T(1024)(128)(2,1)}, u32[]{:S(2)}) copy-start(bf16[2048]{0:T(1024)(128)(2,1)} %param.29) | copy-start | bytes 12292
  146.0 4.0 %copy-start.4 = (bf16[2048]{0:T(1024)(128)(2,1)S(1)}, bf16[2048]{0:T(1024)(128)(2,1)}, u32[]{:S(2)}) copy-start(bf16[2048]{0:T(1024)(128)(2,1)} %param.30) | copy-start | bytes 12292
  146.0 31.7 %copy-start.2 = (bf16[64,2048]{1,0:T(8,128)(2,1)S(1)}, bf16[64,2048]{1,0:T(8,128)(2,1)}, u32[]{:S(2)}) copy-start(bf16[64,2048]{1,0:T(8,128)(2,1)} %param.19) | copy-start | bytes 786436
  179.0 0.7 copy-start.1
  180.6 8.9 %all-to-all-start = ((bf16[64,4,512]{2,0,1:T(8,128)(2,1)}), bf16[64,4,512]{2,0,1:T(8,128)(2,1)S(1)}, u32[]{:S(2)}, u32[]{:S(2)}) async-start(bf16[64,4,512]{2,0,1:T(8,128)(2,1)} %bitcast.128), calls=%async_computation.1 | async-start | bytes 524288 | tf_op jit(solution)/shard_map/all_to_all | solution.py:171
  184.0 68.3 %all-gather.14.cloned.1.call-start = ((), (), s32[]{:S(2)}) async-start(), calls=%async_computation.11 | async-start | bytes 3276800 | tf_op jit(solution)/shard_map/all_gather | solution.py:176
  215.1 96.7 %reduce-scatter.5.cloned.1.call-start = ((), (), s32[]{:S(2)}) async-start(), calls=%async_computation.12 | async-start | bytes 3276800 | tf_op jit(solution)/shard_map/reduce_scatter | solution.py:185
  272.0 56.6 %copy-start.6 = (f32[256,2]{0,1:T(2,128)S(1)}, f32[256,2]{0,1:T(2,128)}, u32[]{:S(2)}) copy-start(f32[256,2]{0,1:T(2,128)} %param.32) | copy-start | bytes 6148
  323.9 22.7 %all-to-all-start.2 = ((bf16[8,512,1,80]{1,3,2,0:T(8,128)(2,1)}), bf16[8,512,1,80]{1,3,2,0:T(8,128)(2,1)S(1)}, u32[]{:S(2)}, u32[]{:S(2)}) async-start(bf16[8,512,1,80]{1,3,2,0:T(8,128)(2,1)} %fusion.42), calls=%async_computation.4 | async-start | bytes 1310720 | tf_op jit(solution)/shard_map/all_to_all | solution.py:12
Sparse Core Ops, SparseCore 0:
  8.9 26.9 all-gather.5
  37.5 23.6 all-gather.7
  62.8 29.3 all-gather.9
  93.6 29.6 all-gather.11
  149.6 26.9 reduce-scatter.2
  215.2 37.1 all-gather.13
  272.2 39.5 reduce-scatter.4
